TPU v7x, 32 devices: a whole 2x2x4 slice. The times are simulated.
32 devices in a mesh: fs: 16 (over z, y, core), tp: 2 (over x).
Axes of the slice: x: 2, y: 2, z: 4, core: 2. Of those that a mesh axis runs over, the one named last changes fastest.
Arguments:
- inputs: bfloat16 [32768, 2048], P('fs'), may hold values from -6 to 6
- key_grads: bfloat16 [32768, 1024], P('fs', 'tp'), may hold values from -0.078125 to 0.078125
- weights: float32 [2048, 1024], P('fs', 'tp'), may hold values from -6 to 6
- momentum: float32 [2048, 1024], P('fs', 'tp'), may hold values from -6 to 6
- left_stat: float32 [4, 2048, 2048], P('tp', 'fs'), may hold values from -96 to 96
- right_stat: float32 [8, 128, 128], P('tp'), may hold values from -256 to 256
- left_root: bfloat16 [4, 2048, 2048], P('tp', 'fs'), may hold values from -0.125 to 0.125
- right_root: bfloat16 [8, 128, 128], P('tp'), may hold values from -0.5 to 0.5
Outputs:
- momentum_next: float32 [2048, 1024], P('fs', 'tp')
- left_next: float32 [4, 2048, 2048], P('tp', 'fs')
- right_next: float32 [8, 128, 128], P('tp')
- update: float32 [2048, 1024], P('fs', 'tp')
- weights_next: float32 [2048, 1024], P('fs', 'tp')
- weights_copy: bfloat16 [2048, 1024], P(None, 'tp')
All inputs are finite; a program needn't handle non-finite values.
Results may differ from a plain program's by a relative error of at most 0.0033.
Values may be sent and summed in bfloat16 or wider, within the bound.
A program may use at most 64 MiB of HBM per device.

v0:
```python
import jax
import jax.numpy as jnp
from jax import lax
from jax.sharding import PartitionSpec as P


def body(inputs, key_grads, weights, momentum, left_stat, right_stat, left_root, right_root):
    row_count = weights.shape[0]
    col_count = weights.shape[1]
    block_count = left_root.shape[0]
    head_count = right_root.shape[0]
    head_size = right_root.shape[1]
    model_width = inputs.shape[1]
    partial_grad = lax.dot_general(
        inputs, key_grads, (((0,), (0,)), ((), ())), preferred_element_type=jnp.float32
    )
    summed = lax.psum(partial_grad, "fs")
    whole_bf = summed.astype(jnp.bfloat16)
    row_offset = lax.axis_index("fs") * row_count
    grad = lax.dynamic_slice_in_dim(summed, row_offset, row_count, 0)
    own_rows = lax.dynamic_slice_in_dim(whole_bf, row_offset, row_count, 0)
    whole_blocks = whole_bf.reshape(model_width, block_count, -1)
    left_part = jnp.einsum(
        "brd,dbc->rbc", left_root, whole_blocks, preferred_element_type=jnp.float32
    ).reshape(row_count, col_count)
    row_gram = jnp.einsum(
        "rbc,dbc->brd",
        own_rows.reshape(row_count, block_count, -1),
        whole_blocks,
        preferred_element_type=jnp.float32,
    )
    whole_heads = whole_bf.reshape(model_width, head_count, head_size)
    head_gram = jnp.einsum(
        "dhi,dhj->hij", whole_heads, whole_heads, preferred_element_type=jnp.float32
    )
    left_bf = left_part.astype(jnp.bfloat16)
    precond = jnp.einsum(
        "rhi,hij->rhj",
        left_bf.reshape(row_count, head_count, head_size),
        right_root,
        preferred_element_type=jnp.float32,
    ).reshape(row_count, col_count)
    left_next = 0.95 * left_stat + 0.05 * row_gram
    right_next = 0.95 * right_stat + 0.05 * head_gram
    grad_square, precond_square = lax.psum(
        (jnp.sum(grad * grad), jnp.sum(precond * precond)), ("fs", "tp")
    )
    scale = jnp.sqrt(grad_square / (precond_square + 1e-06))
    momentum_next = 0.9 * momentum + scale * precond
    update = -0.25 * (momentum_next + 0.4 * weights)
    weights_next = weights + update
    weights_copy = lax.all_gather(weights_next.astype(jnp.bfloat16), "fs", axis=0, tiled=True)
    return (momentum_next, left_next, right_next, update, weights_next, weights_copy)


def solution(mesh):
    in_specs = (
        P("fs", None),
        P("fs", "tp"),
        P("fs", "tp"),
        P("fs", "tp"),
        P("tp", "fs", None),
        P("tp", None, None),
        P("tp", "fs", None),
        P("tp", None, None),
    )
    out_specs = (
        P("fs", "tp"),
        P("tp", "fs", None),
        P("tp", None, None),
        P("fs", "tp"),
        P("fs", "tp"),
        P(None, "tp"),
    )
    return jax.shard_map(body, mesh=mesh, in_specs=in_specs, out_specs=out_specs, check_vma=False)
```

profile of v0, /device:TPU:0, one launch (start us, length us, event | category | flops | bytes accessed | tf_op | source)
XLA Modules:
  0.0 232.3 jit_solution(892505422793026913)
XLA Ops:
  7.2 0.0 copy-start
  7.2 0.0 all-reduce.3.cloned.1.call-start
  7.2 1.5 copy-done
  8.8 9.8 %fusion.19 = f32[2048,512]{1,0:T(8,128)} fusion(bf16[2048,2048]{1,0:T(8,128)(2,1)} %param.8, bf16[2048,512]{1,0:T(8,128)(2,1)S(1)} %copy-done), kind=kOutput, calls=%fused_computation.20 | convolution fusion | flops 4294967296 | bytes 14680064 | tf_op jit(solution)/shard_map/dot_general | solution.py:14
  18.6 0.0 all-reduce.3.cloned.1.call-update
  18.6 0.0 all-gather.2.cloned.1.call-start
  18.6 113.9 %all-reduce.3.cloned.1.call-done = f32[2048,512]{1,0:T(8,128)} async-done(((f32[2048,512]{1,0:T(8,128)}), f32[2048,512]{1,0:T(8,128)}) %all-reduce.3.cloned.1.call-update) | async-done | bytes 4194320 | tf_op jit(solution)/shard_map/psum | solution.py:17
  132.6 0.0 copy-start.8
  132.6 2.5 %convert_element_type.16 = bf16[2048,512]{1,0:T(8,128)(2,1)S(1)} convert(f32[2048,512]{1,0:T(8,128)} %all-reduce.3.cloned.1.call-done) | non-fusion elementwise | flops 1048576 | bytes 6291456 | tf_op jit(solution)/shard_map/convert_element_type | solution.py:18
  135.1 0.0 copy-start.1
  135.1 0.0 copy-start.7
  135.2 0.0 copy-done.8
  135.2 0.0 copy-start.5
  135.2 0.0 copy-start.6
  135.2 0.9 fusion.15
  136.1 0.1 copy-done.7
  136.2 0.0 copy-start.4
  136.2 0.9 multiply_reduce_fusion
  137.1 0.0 copy-done.1
  137.1 1.6 multiply_reduce_fusion.1
  138.7 39.7 %all-reduce = (f32[]{:T(128)}, f32[]{:T(128)}) all-reduce(f32[]{:T(128)} %multiply_reduce_fusion.1, f32[]{:T(128)} %get-tuple-element.12), channel_id=1, replica_groups=mesh['fs'=16,'tp'=2] {'fs','tp'}, use_global_device_ids=true, to_apply=%region_2.0 | all-reduce | flops 2 | bytes 16 | tf_op jit(solution)/shard_map/psum | solution.py:45
  179.8 0.1 copy.24
  179.9 0.0 copy-done.5
  179.9 0.0 copy-done.6
  179.9 1.0 fusion.18
  181.0 0.0 all-gather.2.cloned.1.call-update
  181.0 0.9 constant_dynamic-slice_fusion
  181.9 0.1 copy.25
  182.0 0.0 copy-done.4
  182.0 0.0 copy-start.2
  182.1 0.0 copy-start.3
  182.1 5.6 %fusion.12 = f32[4,128,128]{2,1,0:T(8,128)} fusion(f32[4,128,128]{2,1,0:T(8,128)S(1)} %copy-done.4, f32[2048,512]{1,0:T(8,128)} %all-reduce.3.cloned.1.call-done), kind=kOutput, calls=%fused_computation.11 | convolution fusion | flops 269680640 | bytes 4718592 | tf_op jit(solution)/shard_map/dhi,dhj->hij/dot_general | solution.py:33
  187.7 0.0 copy-done.2
  187.7 0.0 copy-done.3
  187.7 2.2 fusion
  189.9 32.6 %all-gather.2.cloned.1.call-done = bf16[2048,512]{1,0:T(8,128)(2,1)} async-done(((bf16[128,512]{1,0:T(8,128)(2,1)}), bf16[2048,512]{1,0:T(8,128)(2,1)}) %all-gather.2.cloned.1.call-update) | async-done | bytes 2097168 | tf_op jit(solution)/shard_map/all_gather | solution.py:52
  222.4 3.0 %copy.55 = bf16[2048,512]{1,0:T(8,128)(2,1)} copy(bf16[2048,512]{1,0:T(8,128)(2,1)} %all-gather.2.cloned.1.call-done) | data formatting | bytes 4194304
  (1 shorter events, 0.0 us)
Async XLA Ops:
  7.2 1.6 copy-start
  7.2 125.4 %all-reduce.3.cloned.1.call-start = ((), (), s32[]{:S(2)}) async-start(), calls=%async_computation | async-start | bytes 8388608 | tf_op jit(solution)/shard_map/psum | solution.py:17
  18.6 203.8 %all-gather.2.cloned.1.call-start = ((), (), s32[]{:S(2)}) async-start(), calls=%async_computation.1 | async-start | bytes 2228224 | tf_op jit(solution)/shard_map/all_gather | solution.py:52
  132.6 2.6 %copy-start.8 = (bf16[2,128,2048]{2,1,0:T(8,128)(2,1)S(1)}, bf16[2,128,2048]{2,1,0:T(8,128)(2,1)}, u32[]{:S(2)}) copy-start(bf16[2,128,2048]{2,1,0:T(8,128)(2,1)} %param.14) | copy-start | bytes 3145732
  135.1 1.9 copy-start.1
  135.1 1.0 copy-start.7
  135.2 44.7 %copy-start.5 = (f32[128,512]{1,0:T(8,128)S(1)}, f32[128,512]{1,0:T(8,128)}, u32[]{:S(2)}) copy-start(f32[128,512]{1,0:T(8,128)} %param.10) | copy-start | bytes 786436
  135.2 44.7 %copy-start.6 = (f32[128,512]{1,0:T(8,128)S(1)}, f32[128,512]{1,0:T(8,128)}, u32[]{:S(2)}) copy-start(f32[128,512]{1,0:T(8,128)} %param.11) | copy-start | bytes 786436
  136.2 45.8 %copy-start.4 = (f32[4,128,128]{2,1,0:T(8,128)S(1)}, f32[4,128,128]{2,1,0:T(8,128)}, u32[]{:S(2)}) copy-start(f32[4,128,128]{2,1,0:T(8,128)} %param.13) | copy-start | bytes 786436
  182.0 5.6 %copy-start.2 = (bf16[2048,512]{1,0:T(8,128)(2,1)S(1)}, bf16[2048,512]{1,0:T(8,128)(2,1)}, u32[]{:S(2)}) copy-start(bf16[2048,512]{1,0:T(8,128)(2,1)} %copy-done.1) | copy-start | bytes 6291460
  182.1 5.6 %copy-start.3 = (f32[2,128,2048]{2,1,0:T(8,128)S(1)}, f32[2,128,2048]{2,1,0:T(8,128)}, u32[]{:S(2)}) copy-start(f32[2,128,2048]{2,1,0:T(8,128)} %param.12) | copy-start | bytes 6291460
Sparse Core Ops, SparseCore 0:
  18.7 113.8 all-reduce.2
  181.1 41.2 all-gather.1
where the time goes:
time: 233 us; the launch traced here: 232 us
  waiting for transfers between devices  147 us (63%)
  blocking collectives  39.7 us (17%)
  matrix products  19.4 us (8%)
  between operations  15.5 us (7%)
  local copies, waits for them, and re-layouts  5.87 us (3%)
  other arithmetic  5.21 us (2%)
    psum x1, waiting for transfers between devices, body(): summed = lax.psum(partial_grad, 'fs')  114 us
    psum x1, blocking collectives, body(): lax.psum((jnp.sum(grad * grad), jnp.sum(precond * precond)), ('fs', 'tp'))  39.7 us
    all_gather x1, waiting for transfers between devices, body(): lax.all_gather(weights_next.astype(jnp.bfloat16), 'fs', axis=0, tiled=True)  32.6 us
    dot_general x1, matrix products, body(): lax.dot_general(inputs, key_grads, (((0,), (0,)), ((), ())), preferred_el...  9.81 us
    dot_general x1, matrix products, body(): jnp.einsum('dhi,dhj->hij', whole_heads, whole_heads, preferred_element_ty...  5.61 us
    unnamed x19, local copies, waits for them, and re-layouts  4.7 us
  transfers between devices with their start and end apart: 2, of which 2 were waited for; matrix products, arithmetic and copies ran while one was open for 4% of the time, Pallas kernels for 0%

commit v1 on v0

--- a/solution.py
+++ b/solution.py
@@ -14,7 +14,11 @@
     partial_grad = lax.dot_general(
         inputs, key_grads, (((0,), (0,)), ((), ())), preferred_element_type=jnp.float32
     )
-    summed = lax.psum(partial_grad, "fs")
+    width = lax.axis_size("fs")
+    summed = partial_grad
+    for dev_i in [[(dev, dev ^ m) for dev in range(width)] for m in (1, 2, 4, 8, 16) if m < width]:
+        back = lax.ppermute(summed, "fs", dev_i)
+        summed = summed + back
     whole_bf = summed.astype(jnp.bfloat16)
     row_offset = lax.axis_index("fs") * row_count
     grad = lax.dynamic_slice_in_dim(summed, row_offset, row_count, 0)

time: 233 us -> 498 us (2.14)
  waiting for transfers between devices: 147 us -> 403 us
  starting transfers between devices: 0.08 us -> 7.93 us
  other arithmetic: 5.21 us -> 11.5 us
  matrix products: 19.4 us -> 14.3 us
    ppermute x0 -> x4, waiting for transfers between devices: none -> 368 us  [body(): back = lax.ppermute(summed, 'fs', dev_i)]
    psum x1 -> x0, waiting for transfers between devices: 114 us -> none  [body(): summed = lax.psum(partial_grad, 'fs')]
    ppermute x0 -> x4, starting transfers between devices: none -> 7.89 us  [body(): back = lax.ppermute(summed, 'fs', dev_i)]
  transfers between devices with their start and end apart: 2 -> 5, of which waited for: 2 -> 5; matrix products, arithmetic and copies ran while one was open for 4% -> 1% of each run, Pallas kernels for 0% -> 0%
where the time goes in v1:
time: 498 us
  waiting for transfers between devices  403 us (81%)
  blocking collectives  39.7 us (8%)
  between operations  15.5 us (3%)
  matrix products  14.3 us (3%)
  other arithmetic  11.5 us (2%)
  starting transfers between devices  7.93 us (2%)
  local copies, waits for them, and re-layouts  5.68 us (1%)
    ppermute x4, waiting for transfers between devices, body(): back = lax.ppermute(summed, 'fs', dev_i)  368 us
    psum x1, blocking collectives, body(): lax.psum((jnp.sum(grad * grad), jnp.sum(precond * precond)), ('fs', 'tp'))  39.7 us
    all_gather x1, waiting for transfers between devices, body(): lax.all_gather(weights_next.astype(jnp.bfloat16), 'fs', axis=0, tiled=True)  35.5 us
  transfers between devices with their start and end apart: 5, of which 5 were waited for; matrix products, arithmetic and copies ran while one was open for 1% of the time, Pallas kernels for 0%

profile of v1, /device:TPU:0, one launch (start us, length us, event | category | flops | bytes accessed | tf_op | source)
XLA Modules:
  0.0 497.7 jit_solution(17114781595051486600)
XLA Ops:
  7.2 0.0 copy-start
  7.2 0.0 all-gather.2.cloned.1.call-start
  7.2 1.5 copy-done
  8.8 6.9 %fusion.4 = f32[2048,512]{0,1:T(8,128)S(1)} fusion(bf16[2048,2048]{1,0:T(8,128)(2,1)} %param.8, bf16[2048,512]{1,0:T(8,128)(2,1)S(1)} %copy-done), kind=kOutput, calls=%fused_computation.13 | convolution fusion | flops 4294967296 | bytes 14680064 | tf_op jit(solution)/shard_map/dot_general | solution.py:14
  15.7 0.6 collective-permute-start
  16.3 6.8 %collective-permute-done = f32[2048,512]{0,1:T(8,128)S(1)} collective-permute-done((f32[2048,512]{0,1:T(8,128)S(1)}, f32[2048,512]{0,1:T(8,128)S(1)}, u32[]{:S(2)}, u32[]{:S(2)}) %collective-permute-start) | collective-permute-done | bytes 4194336 | tf_op jit(solution)/shard_map/ppermute | solution.py:20
  23.1 1.1 add.38
  24.1 2.9 collective-permute-start.1
  27.1 90.9 %collective-permute-done.1 = f32[2048,512]{0,1:T(8,128)S(1)} collective-permute-done((f32[2048,512]{0,1:T(8,128)S(1)}, f32[2048,512]{0,1:T(8,128)S(1)}, u32[]{:S(2)}, u32[]{:S(2)}) %collective-permute-start.1) | collective-permute-done | bytes 4194336 | tf_op jit(solution)/shard_map/ppermute | solution.py:20
  118.0 1.1 add.39
  119.0 1.9 collective-permute-start.2
  120.9 90.2 %collective-permute-done.2 = f32[2048,512]{0,1:T(8,128)S(1)} collective-permute-done((f32[2048,512]{0,1:T(8,128)S(1)}, f32[2048,512]{0,1:T(8,128)S(1)}, u32[]{:S(2)}, u32[]{:S(2)}) %collective-permute-start.2) | collective-permute-done | bytes 4194336 | tf_op jit(solution)/shard_map/ppermute | solution.py:20
  211.1 2.7 add.40
  213.9 2.5 collective-permute-start.3
  216.4 0.0 copy-start.8
  216.4 179.7 %collective-permute-done.3 = f32[2048,512]{0,1:T(8,128)} collective-permute-done((f32[2048,512]{0,1:T(8,128)}, f32[2048,512]{0,1:T(8,128)}, u32[]{:S(2)}, u32[]{:S(2)}) %collective-permute-start.3) | collective-permute-done | bytes 4194336 | tf_op jit(solution)/shard_map/ppermute | solution.py:20
  396.1 4.9 fusion.3
  401.0 0.0 copy-start.1
  401.0 0.0 copy-start.7
  401.1 0.7 multiply_reduce_fusion.1
  401.7 0.0 copy-done.8
  401.7 0.0 copy-start.5
  401.7 0.0 copy-start.6
  401.7 0.7 convolution_convert_fusion
  402.4 0.0 copy-start.4
  402.5 0.0 copy-done.7
  402.5 0.9 multiply_reduce_fusion
  403.3 0.0 copy-done.1
  403.3 39.7 %all-reduce = (f32[]{:T(128)}, f32[]{:T(128)}) all-reduce(f32[]{:T(128)} %multiply_reduce_fusion.1, f32[]{:T(128)} %get-tuple-element.14), channel_id=1, replica_groups=mesh['fs'=16,'tp'=2] {'fs','tp'}, use_global_device_ids=true, to_apply=%region_1.0 | all-reduce | flops 2 | bytes 16 | tf_op jit(solution)/shard_map/psum | solution.py:49
  444.4 0.1 copy.21
  444.5 0.0 copy-done.5
  444.5 0.0 copy-done.6
  444.5 1.0 fusion.2
  445.5 0.0 all-gather.2.cloned.1.call-update
  445.6 0.9 constant_dynamic-slice_fusion
  446.5 0.0 copy-done.4
  446.5 0.0 copy-start.2
  446.5 0.0 copy-start.3
  446.5 3.8 fusion.1
  450.3 0.0 copy-done.2
  450.3 0.0 copy-done.3
  450.3 2.0 fusion
  452.3 35.5 %all-gather.2.cloned.1.call-done = bf16[2048,512]{1,0:T(8,128)(2,1)} async-done(((bf16[128,512]{1,0:T(8,128)(2,1)}), bf16[2048,512]{1,0:T(8,128)(2,1)}) %all-gather.2.cloned.1.call-update) | async-done | bytes 2097168 | tf_op jit(solution)/shard_map/all_gather | solution.py:56
  487.8 3.0 copy.31
  (1 shorter events, 0.0 us)
Async XLA Ops:
  7.2 1.6 copy-start
  7.2 480.6 %all-gather.2.cloned.1.call-start = ((), (), s32[]{:S(2)}) async-start(), calls=%async_computation | async-start | bytes 2228224 | tf_op jit(solution)/shard_map/all_gather | solution.py:56
  15.7 7.3 %collective-permute-start = (f32[2048,512]{0,1:T(8,128)S(1)}, f32[2048,512]{0,1:T(8,128)S(1)}, u32[]{:S(2)}, u32[]{:S(2)}) collective-permute-start(f32[2048,512]{0,1:T(8,128)S(1)} %fusion.4), channel_id=1, source_target_pairs={{0,2},{2,0},{4,6},{6,4},{8,10},{10,8},{12,14},{14,12},{16,18},{18,... | collective-permute-start | bytes 12582920 | tf_op jit(solution)/shard_map/ppermute | solution.py:20
  24.1 93.8 %collective-permute-start.1 = (f32[2048,512]{0,1:T(8,128)S(1)}, f32[2048,512]{0,1:T(8,128)S(1)}, u32[]{:S(2)}, u32[]{:S(2)}) collective-permute-start(f32[2048,512]{0,1:T(8,128)S(1)} %add.38), channel_id=1, source_target_pairs={{0,4},{2,6},{4,0},{6,2},{8,12},{10,14},{12,8},{14,10},{16,20},{18,... | collective-permute-start | bytes 12582920 | tf_op jit(solution)/shard_map/ppermute | solution.py:20
  119.0 92.1 %collective-permute-start.2 = (f32[2048,512]{0,1:T(8,128)S(1)}, f32[2048,512]{0,1:T(8,128)S(1)}, u32[]{:S(2)}, u32[]{:S(2)}) collective-permute-start(f32[2048,512]{0,1:T(8,128)S(1)} %add.39), channel_id=1, source_target_pairs={{0,8},{2,10},{4,12},{6,14},{8,0},{10,2},{12,4},{14,6},{16,24},{18,... | collective-permute-start | bytes 12582920 | tf_op jit(solution)/shard_map/ppermute | solution.py:20
  213.9 182.3 %collective-permute-start.3 = (f32[2048,512]{0,1:T(8,128)}, f32[2048,512]{0,1:T(8,128)}, u32[]{:S(2)}, u32[]{:S(2)}) collective-permute-start(f32[2048,512]{0,1:T(8,128)} %add.40), channel_id=1, source_target_pairs={{0,16},{2,18},{4,20},{6,22},{8,24},{10,26},{12,28},{14,30},{16,0},... | collective-permute-start | bytes 12582920 | tf_op jit(solution)/shard_map/ppermute | solution.py:20
  216.4 185.3 %copy-start.8 = (bf16[2,128,2048]{2,1,0:T(8,128)(2,1)S(1)}, bf16[2,128,2048]{2,1,0:T(8,128)(2,1)}, u32[]{:S(2)}) copy-start(bf16[2,128,2048]{2,1,0:T(8,128)(2,1)} %param.14) | copy-start | bytes 3145732
  401.0 2.3 copy-start.1
  401.0 1.4 copy-start.7
  401.7 42.8 %copy-start.5 = (f32[128,512]{1,0:T(8,128)S(1)}, f32[128,512]{1,0:T(8,128)}, u32[]{:S(2)}) copy-start(f32[128,512]{1,0:T(8,128)} %param.10) | copy-start | bytes 786436
  401.7 42.8 %copy-start.6 = (f32[128,512]{1,0:T(8,128)S(1)}, f32[128,512]{1,0:T(8,128)}, u32[]{:S(2)}) copy-start(f32[128,512]{1,0:T(8,128)} %param.11) | copy-start | bytes 786436
  402.4 44.0 %copy-start.4 = (f32[4,128,128]{2,1,0:T(8,128)S(1)}, f32[4,128,128]{2,1,0:T(8,128)}, u32[]{:S(2)}) copy-start(f32[4,128,128]{2,1,0:T(8,128)} %param.13) | copy-start | bytes 786436
  446.5 3.8 copy-start.2
  446.5 3.8 copy-start.3
Sparse Core Ops, SparseCore 0:
  445.7 42.0 all-gather.1

commit v2 on v0

--- a/solution.py
+++ b/solution.py
@@ -49,7 +49,9 @@
     momentum_next = 0.9 * momentum + scale * precond
     update = -0.25 * (momentum_next + 0.4 * weights)
     weights_next = weights + update
-    weights_copy = lax.all_gather(weights_next.astype(jnp.bfloat16), "fs", axis=0, tiled=True)
+    part = weights_next.astype(jnp.bfloat16)
+    outgoing = jnp.stack([part] * lax.axis_size("fs"))
+    weights_copy = jnp.concatenate(lax.all_to_all(outgoing, "fs", 0, 0), axis=0)
     return (momentum_next, left_next, right_next, update, weights_next, weights_copy)
 
 

time: 233 us -> 245 us (1.052)
  the two profiles are of different devices: /device:TPU:0 before, /device:TPU:13 now
where the time goes in v2:
time: 245 us
  waiting for transfers between devices  150 us (61%)
  blocking collectives  39.8 us (16%)
  matrix products  19.4 us (8%)
  between operations  15.5 us (6%)
  local copies, waits for them, and re-layouts  7.42 us (3%)
  starting transfers between devices  7.35 us (3%)
  other arithmetic  5.18 us (2%)
    psum x1, waiting for transfers between devices, body(): summed = lax.psum(partial_grad, 'fs')  111 us
    psum x1, blocking collectives, body(): lax.psum((jnp.sum(grad * grad), jnp.sum(precond * precond)), ('fs', 'tp'))  39.8 us
    all_to_all x1, waiting for transfers between devices, body(): weights_copy = jnp.concatenate(lax.all_to_all(outgoing, 'fs', 0, 0), axis=0)  38.7 us
    dot_general x1, matrix products, body(): lax.dot_general(inputs, key_grads, (((0,), (0,)), ((), ())), preferred_el...  9.81 us
    all_to_all x1, starting transfers between devices, body(): weights_copy = jnp.concatenate(lax.all_to_all(outgoing, 'fs', 0, 0), axis=0)  7.31 us
    dot_general x1, matrix products, body(): jnp.einsum('dhi,dhj->hij', whole_heads, whole_heads, preferred_element_ty...  5.62 us
  transfers between devices with their start and end apart: 2, of which 2 were waited for; matrix products, arithmetic and copies ran while one was open for 4% of the time, Pallas kernels for 0%

profile of v2, /device:TPU:13, one launch (start us, length us, event | category | flops | bytes accessed | tf_op | source)
XLA Modules:
  0.0 244.5 jit_solution(11632135612856630964)
XLA Ops:
  7.2 0.0 copy-start
  7.2 0.0 all-reduce.3.cloned.1.call-start
  7.2 1.5 copy-done
  8.8 9.8 %fusion.19 = f32[2048,512]{1,0:T(8,128)} fusion(bf16[2048,2048]{1,0:T(8,128)(2,1)} %param.8, bf16[2048,512]{1,0:T(8,128)(2,1)S(1)} %copy-done), kind=kOutput, calls=%fused_computation.20 | convolution fusion | flops 4294967296 | bytes 14680064 | tf_op jit(solution)/shard_map/dot_general | solution.py:14
  18.6 0.0 all-reduce.3.cloned.1.call-update
  18.6 111.2 %all-reduce.3.cloned.1.call-done = f32[2048,512]{1,0:T(8,128)} async-done(((f32[2048,512]{1,0:T(8,128)}), f32[2048,512]{1,0:T(8,128)}) %all-reduce.3.cloned.1.call-update) | async-done | bytes 4194320 | tf_op jit(solution)/shard_map/psum | solution.py:17
  129.9 0.0 copy-start.8
  129.9 2.5 %convert_element_type.16 = bf16[2048,512]{1,0:T(8,128)(2,1)S(1)} convert(f32[2048,512]{1,0:T(8,128)} %all-reduce.3.cloned.1.call-done) | non-fusion elementwise | flops 1048576 | bytes 6291456 | tf_op jit(solution)/shard_map/convert_element_type | solution.py:18
  132.4 0.0 copy-start.1
  132.4 0.0 copy-start.7
  132.4 0.0 copy-done.8
  132.4 0.0 copy-start.5
  132.4 0.0 copy-start.6
  132.5 0.9 fusion.15
  133.4 0.1 copy-done.7
  133.5 0.9 multiply_reduce_fusion
  134.3 0.0 copy-done.1
  134.3 1.6 multiply_reduce_fusion.1
  136.0 39.8 %all-reduce = (f32[]{:T(128)}, f32[]{:T(128)}) all-reduce(f32[]{:T(128)} %multiply_reduce_fusion.1, f32[]{:T(128)} %get-tuple-element.12), channel_id=1, replica_groups=mesh['fs'=16,'tp'=2] {'fs','tp'}, use_global_device_ids=true, to_apply=%region_2.0 | all-reduce | flops 2 | bytes 16 | tf_op jit(solution)/shard_map/psum | solution.py:45
  177.1 0.1 copy.24
  177.2 0.0 copy-done.5
  177.2 0.0 copy-done.6
  177.3 1.0 fusion.18
  178.3 1.6 stack.2
  179.8 0.0 copy-start.4
  179.8 7.3 %all-to-all-start = ((bf16[16,128,512]{2,1,0:T(8,128)(2,1)}), bf16[16,128,512]{2,1,0:T(8,128)(2,1)}, u32[]{:S(2)}, u32[]{:S(2)}) async-start(bf16[16,128,512]{2,1,0:T(8,128)(2,1)} %stack.2), calls=%async_computation | async-start | bytes 4194304 | tf_op jit(solution)/shard_map/all_to_all | solution.py:54
  187.1 0.9 constant_dynamic-slice_fusion
  188.0 0.1 copy.25
  188.2 0.0 copy-done.4
  188.2 0.0 copy-start.2
  188.2 0.0 copy-start.3
  188.2 5.6 %fusion.12 = f32[4,128,128]{2,1,0:T(8,128)} fusion(f32[4,128,128]{2,1,0:T(8,128)S(1)} %copy-done.4, f32[2048,512]{1,0:T(8,128)} %all-reduce.3.cloned.1.call-done), kind=kOutput, calls=%fused_computation.11 | convolution fusion | flops 269680640 | bytes 4718592 | tf_op jit(solution)/shard_map/dhi,dhj->hij/dot_general | solution.py:33
  193.8 0.0 copy-done.2
  193.8 0.0 copy-done.3
  193.8 2.2 fusion
  196.0 38.7 %all-to-all-done = bf16[16,128,512]{2,1,0:T(8,128)(2,1)} async-done(((bf16[16,128,512]{2,1,0:T(8,128)(2,1)}), bf16[16,128,512]{2,1,0:T(8,128)(2,1)}, u32[]{:S(2)}, u32[]{:S(2)}) %all-to-all-start) | async-done | bytes 2097184 | tf_op jit(solution)/shard_map/all_to_all | solution.py:54
  234.7 3.0 %copy.55 = bf16[2048,512]{1,0:T(8,128)(2,1)} copy(bf16[2048,512]{1,0:T(8,128)(2,1)} %bitcast.5) | data formatting | bytes 4194304
  (1 shorter events, 0.0 us)
Async XLA Ops:
  7.2 1.6 copy-start
  7.2 122.7 %all-reduce.3.cloned.1.call-start = ((), (), s32[]{:S(2)}) async-start(), calls=%async_computation.1 | async-start | bytes 8388608 | tf_op jit(solution)/shard_map/psum | solution.py:17
  129.9 2.6 %copy-start.8 = (bf16[2,128,2048]{2,1,0:T(8,128)(2,1)S(1)}, bf16[2,128,2048]{2,1,0:T(8,128)(2,1)}, u32[]{:S(2)}) copy-start(bf16[2,128,2048]{2,1,0:T(8,128)(2,1)} %param.14) | copy-start | bytes 3145732
  132.4 1.9 copy-start.1
  132.4 1.0 copy-start.7
  132.4 44.8 %copy-start.5 = (f32[128,512]{1,0:T(8,128)S(1)}, f32[128,512]{1,0:T(8,128)}, u32[]{:S(2)}) copy-start(f32[128,512]{1,0:T(8,128)} %param.10) | copy-start | bytes 786436
  132.4 44.8 %copy-start.6 = (f32[128,512]{1,0:T(8,128)S(1)}, f32[128,512]{1,0:T(8,128)}, u32[]{:S(2)}) copy-start(f32[128,512]{1,0:T(8,128)} %param.11) | copy-start | bytes 786436
  179.8 8.4 %copy-start.4 = (f32[4,128,128]{2,1,0:T(8,128)S(1)}, f32[4,128,128]{2,1,0:T(8,128)}, u32[]{:S(2)}) copy-start(f32[4,128,128]{2,1,0:T(8,128)} %param.13) | copy-start | bytes 786436
  179.8 54.8 %all-to-all-start = ((bf16[16,128,512]{2,1,0:T(8,128)(2,1)}), bf16[16,128,512]{2,1,0:T(8,128)(2,1)}, u32[]{:S(2)}, u32[]{:S(2)}) async-start(bf16[16,128,512]{2,1,0:T(8,128)(2,1)} %stack.2), calls=%async_computation | async-start | bytes 4194304 | tf_op jit(solution)/shard_map/all_to_all | solution.py:54
  188.2 5.6 %copy-start.2 = (bf16[2048,512]{1,0:T(8,128)(2,1)S(1)}, bf16[2048,512]{1,0:T(8,128)(2,1)}, u32[]{:S(2)}) copy-start(bf16[2048,512]{1,0:T(8,128)(2,1)} %copy-done.1) | copy-start | bytes 6291460
  188.2 5.6 %copy-start.3 = (f32[2,128,2048]{2,1,0:T(8,128)S(1)}, f32[2,128,2048]{2,1,0:T(8,128)}, u32[]{:S(2)}) copy-start(f32[2,128,2048]{2,1,0:T(8,128)} %param.12) | copy-start | bytes 6291460
Sparse Core Ops, SparseCore 0:
  18.7 111.0 all-reduce.2
